TPU v7x, 32 devices: a whole 2x2x4 slice. The times are simulated.
32 devices in a mesh: rep: 2 (over x), fs: 8 (over z, y), tp: 2 (over core).
Axes of the slice: x: 2, y: 2, z: 4, core: 2. Of those that a mesh axis runs over, the one named last changes fastest.
Arguments:
- activations: bfloat16 [3072, 2048], P(('rep', 'fs'), 'tp'), may hold values from -6 to 6
- mix_gain: float32 [2048], replicated, may hold values from 0.1 to 1.9
- mlp_gain: float32 [2048], replicated, may hold values from 0.1 to 1.9
- query_weight: float32 [2048, 512], P('fs', 'tp'), may hold values from -0.125 to 0.125
- query_scale: float32 [512], P('tp'), may hold values from 0.3 to 3
- key_weight: float32 [2048, 512], P('fs', 'tp'), may hold values from -0.125 to 0.125
- key_scale: float32 [512], P('tp'), may hold values from 0.3 to 3
- value_weight: float32 [2048, 1024], P('fs', 'tp'), may hold values from -0.125 to 0.125
- value_scale: float32 [1024], P('tp'), may hold values from 0.3 to 3
- gate_weight: float32 [2048, 1024], P('fs', 'tp'), may hold values from -0.125 to 0.125
- gate_scale: float32 [1024], P('tp'), may hold values from 0.3 to 3
- out_weight: float32 [1024, 2048], P('tp', 'fs'), may hold values from -0.1875 to 0.1875
- out_scale: float32 [2048], P('fs'), may hold values from 0.3 to 3
- up_weight: float32 [2048, 8192], P('fs', 'tp'), may hold values from -0.125 to 0.125
- up_scale: float32 [8192], P('tp'), may hold values from 0.3 to 3
- down_weight: float32 [8192, 2048], P('tp', 'fs'), may hold values from -0.0625 to 0.0625
- down_scale: float32 [2048], P('fs'), may hold values from 0.3 to 3
- log_decay: float32 [8], P('tp'), may hold values from -0.1 to 0, as said below
Outputs:
- result: bfloat16 [3072, 2048], P(('rep', 'fs'), 'tp')
Inputs may be any that keep to these rules, and one draw needn't show every extreme that they name: `log_decay`: negative for every head.
All inputs are finite; a program needn't handle non-finite values.
Results may differ from a plain program's by a relative error of at most 0.023.
Values may be sent and summed in bfloat16 or wider, within the bound.
A program may use at most 128 MiB of HBM per device.

v0:
```python
import jax
import jax.numpy as jnp
from jax import lax
from jax.sharding import PartitionSpec as P

BLOCK = 64
LENGTH = 192


epsilon = 1e-06
rope_base = 10000.0


def rotate(head_rows, positions):
    half = head_rows.shape[-1] // 2
    inverse = 1.0 / rope_base ** jnp.linspace(0.0, 1.0, half, dtype=jnp.float32)
    angles = positions[:, None] * inverse[None, :]
    cosine = jnp.cos(angles)[:, None, :]
    sine = jnp.sin(angles)[:, None, :]
    first = head_rows[..., :half]
    second = head_rows[..., half:]
    return jnp.concatenate(
        [first * cosine - second * sine, first * sine + second * cosine], axis=-1
    )


def retain(query_heads, key_heads, value_heads, log_decay):
    batch, length, heads, width = query_heads.shape
    block_count = length // BLOCK
    highest = lax.Precision.HIGHEST

    def to_blocks(tensor):
        return tensor.reshape(batch, block_count, BLOCK, heads, tensor.shape[-1]).transpose(
            0, 3, 1, 2, 4
        )

    query_blocks = to_blocks(query_heads)
    key_blocks = to_blocks(key_heads)
    value_blocks = to_blocks(value_heads)
    places = jnp.arange(BLOCK, dtype=jnp.float32)
    offsets = places[:, None] - places[None, :]
    inner = jnp.where(
        offsets >= 0, jnp.exp(log_decay[:, None, None] * jnp.maximum(offsets, 0.0)), 0.0
    )
    scores = (
        jnp.einsum("bhntd,bhnsd->bhnts", query_blocks, key_blocks, precision=highest)
        * inner[None, :, None]
    )
    output = jnp.einsum("bhnts,bhnse->bhnte", scores, value_blocks, precision=highest)
    keys_decayed = (
        key_blocks
        * jnp.exp(log_decay[:, None] * (BLOCK - 1.0 - places)[None, :])[None, :, None, :, None]
    )
    increments = jnp.einsum("bhnsd,bhnse->nbhde", keys_decayed, value_blocks, precision=highest)
    carry_decay = jnp.exp(log_decay * BLOCK)[None, :, None, None]

    def advance(state, increment):
        return (carry_decay * state + increment, state)

    initial = jnp.zeros((batch, heads, width, value_heads.shape[-1]), jnp.float32)
    _, states = lax.scan(advance, initial, increments)
    query_decayed = (
        query_blocks * jnp.exp(log_decay[:, None] * (places + 1.0)[None, :])[None, :, None, :, None]
    )
    output = output + jnp.einsum("bhntd,nbhde->bhnte", query_decayed, states, precision=highest)
    return output.transpose(0, 2, 3, 1, 4).reshape(batch, length, heads, value_heads.shape[-1])


def gather_norm(rows, gain):
    whole = lax.all_gather(rows, "tp", axis=1, tiled=True)
    wide = whole.astype(jnp.float32)
    mean_square = jnp.mean(wide * wide, axis=1, keepdims=True)
    return (wide * lax.rsqrt(mean_square + epsilon) * gain).astype(jnp.bfloat16)


def column_terms(weight, scale, hidden):
    partial_value = lax.dot_general(
        weight, hidden, (((0,), (1,)), ((), ())), preferred_element_type=jnp.float32
    )
    return partial_value * scale[:, None]


def on_device(
    activations,
    mix_gain,
    mlp_gain,
    query_weight,
    query_scale,
    key_weight,
    key_scale,
    value_weight,
    value_scale,
    gate_weight,
    gate_scale,
    out_weight,
    out_scale,
    up_weight,
    up_scale,
    down_weight,
    down_scale,
    log_decay,
):
    query_full, key_full, value_full, gate_full, out_full = (
        lax.all_gather(query_weight.astype(jnp.bfloat16), "fs", axis=0, tiled=True),
        lax.all_gather(key_weight.astype(jnp.bfloat16), "fs", axis=0, tiled=True),
        lax.all_gather(value_weight.astype(jnp.bfloat16), "fs", axis=0, tiled=True),
        lax.all_gather(gate_weight.astype(jnp.bfloat16), "fs", axis=0, tiled=True),
        lax.all_gather(out_weight.astype(jnp.bfloat16), "fs", axis=1, tiled=True),
    )
    out_columns, down_columns = (
        lax.all_gather(out_scale, "fs", axis=0, tiled=True),
        lax.all_gather(down_scale, "fs", axis=0, tiled=True),
    )
    normed = gather_norm(activations, mix_gain)
    total_rows = normed.shape[0]
    sequences = total_rows // LENGTH
    heads = log_decay.shape[0]
    query = jnp.dot(normed, query_full, preferred_element_type=jnp.float32) * query_scale
    key_rows = jnp.dot(normed, key_full, preferred_element_type=jnp.float32) * key_scale
    value = jnp.dot(normed, value_full, preferred_element_type=jnp.float32) * value_scale
    gate = jnp.dot(normed, gate_full, preferred_element_type=jnp.float32) * gate_scale
    positions = jnp.arange(LENGTH, dtype=jnp.float32)
    query_heads = rotate(query.reshape(sequences, LENGTH, heads, -1), positions)
    key_heads = rotate(key_rows.reshape(sequences, LENGTH, heads, -1), positions)
    value_heads = value.reshape(sequences, LENGTH, heads, -1)
    retained = retain(query_heads, key_heads, value_heads, log_decay)
    retained = retained * lax.rsqrt(jnp.mean(retained * retained, axis=-1, keepdims=True) + epsilon)
    attended = (retained.reshape(total_rows, -1) * jax.nn.silu(gate)).astype(jnp.bfloat16)
    mixed = lax.psum_scatter(
        column_terms(out_full, out_columns, attended).astype(jnp.bfloat16),
        "tp",
        scatter_dimension=0,
        tiled=True,
    ).astype(jnp.float32)
    first = (activations.astype(jnp.float32) + mixed.T).astype(jnp.bfloat16)
    normed_two = gather_norm(first, mlp_gain)
    up_full, down_full = (
        lax.all_gather(up_weight.astype(jnp.bfloat16), "fs", axis=0, tiled=True),
        lax.all_gather(down_weight.astype(jnp.bfloat16), "fs", axis=1, tiled=True),
    )
    raised = jnp.dot(normed_two, up_full, preferred_element_type=jnp.float32) * up_scale
    hidden = jnp.square(jax.nn.relu(raised)).astype(jnp.bfloat16)
    channel = lax.psum_scatter(
        column_terms(down_full, down_columns, hidden).astype(jnp.bfloat16),
        "tp",
        scatter_dimension=0,
        tiled=True,
    ).astype(jnp.float32)
    return (first.astype(jnp.float32) + channel.T).astype(jnp.bfloat16)


def solution(mesh):
    placed = (
        P(("rep", "fs"), "tp"),
        P(),
        P(),
        P("fs", "tp"),
        P("tp"),
        P("fs", "tp"),
        P("tp"),
        P("fs", "tp"),
        P("tp"),
        P("fs", "tp"),
        P("tp"),
        P("tp", "fs"),
        P("fs"),
        P("fs", "tp"),
        P("tp"),
        P("tp", "fs"),
        P("fs"),
        P("tp"),
    )
    return jax.shard_map(
        on_device, mesh=mesh, in_specs=placed, out_specs=P(("rep", "fs"), "tp"), check_vma=False
    )
```

profile of v0, /device:TPU:0, one launch (start us, length us, event | category | flops | bytes accessed | tf_op | source)
XLA Modules:
  0.0 743.4 jit_solution(15880534284613785428)
XLA Ops:
  6.5 1.7 convert_element_type.68
  8.3 1.6 convert_element_type.69
  10.0 1.8 convert_element_type.70
  12.0 0.8 convert_element_type.71
  12.8 0.8 convert_element_type.73
  13.8 2.5 all_gather.33
  17.0 22.2 %all-gather = f32[8,1,256]{2,1,0:T(1,128)S(1)} all-gather(f32[1,1,256]{2,1,0:T(1,128)S(1)} %bitcast.109), channel_id=1, replica_groups=mesh['rep'=2,'fs'=8,'tp'=2] {'fs'}, dimensions={0}, use_global_device_ids=true | all-gather | bytes 9216 | tf_op jit(solution)/shard_map/all_gather | solution.py:111
  39.2 13.4 %all-gather.10.cloned.1.call-done = bf16[2048,256]{1,0:T(8,128)(2,1)} async-done(((bf16[256,256]{1,0:T(8,128)(2,1)}), bf16[2048,256]{1,0:T(8,128)(2,1)}) %all-gather.10.cloned.1.call-update) | async-done | bytes 1048592 | tf_op jit(solution)/shard_map/all_gather | solution.py:104
  52.6 1.6 convolution_multiply_fusion.7
  54.4 39.3 %all-gather.12.cloned.1.call-done = bf16[2048,256]{1,0:T(8,128)(2,1)} async-done(((bf16[256,256]{1,0:T(8,128)(2,1)}), bf16[2048,256]{1,0:T(8,128)(2,1)}) %all-gather.12.cloned.1.call-update) | async-done | bytes 1048592 | tf_op jit(solution)/shard_map/all_gather | solution.py:105
  93.8 1.6 convolution_multiply_fusion.6
  96.1 0.8 convolution_multiply_fusion.5
  96.8 46.9 %all-gather.14.cloned.1.call-done = bf16[2048,512]{1,0:T(8,128)(2,1)} async-done(((bf16[256,512]{1,0:T(8,128)(2,1)}), bf16[2048,512]{1,0:T(8,128)(2,1)}) %all-gather.14.cloned.1.call-update) | async-done | bytes 2097168 | tf_op jit(solution)/shard_map/all_gather | solution.py:106
  143.7 2.2 convolution_multiply_fusion.4
  146.1 0.9 convolution_bitcast_fusion
  147.5 2.3 while.13
  147.5 0.7 bitcast_dynamic-update-slice_fusion.2
  148.3 0.7 bitcast_dynamic-update-slice_fusion.2
  149.9 1.7 multiply_reduce_fusion
  152.0 41.4 %all-gather.16.cloned.1.call-done = bf16[2048,512]{1,0:T(8,128)(2,1)} async-done(((bf16[256,512]{1,0:T(8,128)(2,1)}), bf16[2048,512]{1,0:T(8,128)(2,1)}) %all-gather.16.cloned.1.call-update) | async-done | bytes 2097168 | tf_op jit(solution)/shard_map/all_gather | solution.py:107
  193.4 50.8 %all-gather.18.cloned.1.call-done = bf16[512,2048]{1,0:T(8,128)(2,1)} async-done(((bf16[512,256]{1,0:T(8,128)(2,1)}), bf16[512,2048]{1,0:T(8,128)(2,1)}) %all-gather.18.cloned.1.call-update) | async-done | bytes 2097168 | tf_op jit(solution)/shard_map/all_gather | solution.py:108
  244.4 4.3 fusion.6
  248.8 3.8 convert_element_type.80
  252.7 3.8 convert_element_type.82
  257.2 17.9 %all-gather.1 = f32[8,1,256]{2,1,0:T(1,128)S(1)} all-gather(f32[1,1,256]{2,1,0:T(1,128)S(1)} %bitcast.110), channel_id=1, replica_groups=mesh['rep'=2,'fs'=8,'tp'=2] {'fs'}, dimensions={0}, use_global_device_ids=true | all-gather | bytes 9216 | tf_op jit(solution)/shard_map/all_gather | solution.py:112
  275.1 1.1 fusion.16
  276.3 2.4 all_gather.40
  278.9 207.0 %all-gather.20.cloned.1.call-done = bf16[2048,4096]{1,0:T(8,128)(2,1)} async-done(((bf16[256,4096]{1,0:T(8,128)(2,1)}), bf16[2048,4096]{1,0:T(8,128)(2,1)}) %all-gather.20.cloned.1.call-update) | async-done | bytes 16777232 | tf_op jit(solution)/shard_map/all_gather | solution.py:138
  485.9 227.6 %all-gather.22.cloned.1.call-done = bf16[4096,2048]{1,0:T(8,128)(2,1)} async-done(((bf16[4096,256]{1,0:T(8,128)(2,1)}), bf16[4096,2048]{1,0:T(8,128)(2,1)}) %all-gather.22.cloned.1.call-update) | async-done | bytes 16777232 | tf_op jit(solution)/shard_map/all_gather | solution.py:139
  713.4 15.1 %fusion.5 = bf16[2048,192]{0,1:T(8,128)(2,1)} fusion(bf16[4096,2048]{1,0:T(8,128)(2,1)} %all-gather.22.cloned.1.call-done, f32[2048]{0:T(1024)S(1)} %bitcast.108, bf16[2048,4096]{1,0:T(8,128)(2,1)} %all-gather.20.cloned.1.call-done, f32[4096]{0:T(1024)S(1)} %copy-done.6, bf16[192,2048]{1,0:T(8,128)(2,1)S(1)} %all_gather.40, f32[2048]{0:T(1024)S(1)} %copy-done.8, ...), kind=kOutput, calls=%fused_computation.10 | convolution fusion | flops 6447955968 | bytes 35160832 | tf_op jit(solution)/shard_map/dot_general | solution.py:77
  728.5 6.5 reduce-scatter.5.cloned.1.call-done
  735.0 1.9 fusion.15
  (76 shorter events, 5.1 us)
Async XLA Ops:
  6.5 5.4 copy-start.1
  6.5 6.3 copy-start.2
  6.5 46.1 %all-gather.10.cloned.1.call-start = ((), (), s32[]{:S(2)}) async-start(), calls=%async_computation.2 | async-start | bytes 1179648 | tf_op jit(solution)/shard_map/all_gather | solution.py:104
  8.3 85.5 %all-gather.12.cloned.1.call-start = ((), (), s32[]{:S(2)}) async-start(), calls=%async_computation.3 | async-start | bytes 1179648 | tf_op jit(solution)/shard_map/all_gather | solution.py:105
  10.0 3.8 copy-start
  10.0 133.7 %all-gather.14.cloned.1.call-start = ((), (), s32[]{:S(2)}) async-start(), calls=%async_computation.4 | async-start | bytes 2359296 | tf_op jit(solution)/shard_map/all_gather | solution.py:106
  11.9 181.5 %all-gather.16.cloned.1.call-start = ((), (), s32[]{:S(2)}) async-start(), calls=%async_computation.5 | async-start | bytes 2359296 | tf_op jit(solution)/shard_map/all_gather | solution.py:107
  12.7 4.1 copy-start.3
  12.7 4.3 copy-start.4
  12.8 39.9 %copy-start.7 = (f32[2048]{0:T(1024)S(1)}, f32[2048]{0:T(1024)}, u32[]{:S(2)}) copy-start(f32[2048]{0:T(1024)} %param.23) | copy-start | bytes 24580
  12.8 39.9 %copy-start.11 = (f32[256]{0:T(256)S(1)}, f32[256]{0:T(256)}, u32[]{:S(2)}) copy-start(f32[256]{0:T(256)} %param.26) | copy-start | bytes 3076
  12.8 231.4 %all-gather.18.cloned.1.call-start = ((), (), s32[]{:S(2)}) async-start(), calls=%async_computation.6 | async-start | bytes 2359296 | tf_op jit(solution)/shard_map/all_gather | solution.py:108
  13.6 261.5 %reduce-scatter.3.cloned.1.call-start = ((), (), s32[]{:S(2)}) async-start(), calls=%async_computation.7 | async-start | bytes 1179648 | tf_op jit(solution)/shard_map/reduce_scatter | solution.py:129
  16.9 76.9 %copy-start.12 = (f32[256]{0:T(256)S(1)}, f32[256]{0:T(256)}, u32[]{:S(2)}) copy-start(f32[256]{0:T(256)} %param.28) | copy-start | bytes 3076
  95.7 48.1 %copy-start.9 = (f32[512]{0:T(512)S(1)}, f32[512]{0:T(512)}, u32[]{:S(2)}) copy-start(f32[512]{0:T(512)} %param.30) | copy-start | bytes 6148
  149.8 94.6 %copy-start.10 = (f32[512]{0:T(512)S(1)}, f32[512]{0:T(512)}, u32[]{:S(2)}) copy-start(f32[512]{0:T(512)} %param.32) | copy-start | bytes 6148
  248.8 237.1 %all-gather.20.cloned.1.call-start = ((), (), s32[]{:S(2)}) async-start(), calls=%async_computation.8 | async-start | bytes 18874368 | tf_op jit(solution)/shard_map/all_gather | solution.py:138
  252.6 460.8 %all-gather.22.cloned.1.call-start = ((), (), s32[]{:S(2)}) async-start(), calls=%async_computation.9 | async-start | bytes 18874368 | tf_op jit(solution)/shard_map/all_gather | solution.py:139
  256.5 0.7 copy-start.5
  256.5 478.5 %reduce-scatter.5.cloned.1.call-start = ((), (), s32[]{:S(2)}) async-start(), calls=%async_computation.10 | async-start | bytes 1179648 | tf_op jit(solution)/shard_map/reduce_scatter | solution.py:143
  275.1 438.3 %copy-start.6 = (f32[4096]{0:T(1024)S(1)}, f32[4096]{0:T(1024)}, u32[]{:S(2)}) copy-start(f32[4096]{0:T(1024)} %param.36) | copy-start | bytes 49156
  275.1 438.3 %copy-start.8 = (f32[2048]{0:T(1024)S(1)}, f32[2048]{0:T(1024)}, u32[]{:S(2)}) copy-start(f32[2048]{0:T(1024)} %param.24) | copy-start | bytes 24580
Sparse Core Ops, SparseCore 0:
  9.5 43.1 all-gather.9
  54.7 38.9 all-gather.11
  95.9 47.7 all-gather.13
  145.7 47.6 all-gather.15
  195.2 48.8 all-gather.17
  248.9 6.3 reduce-scatter.2
  257.4 228.4 all-gather.19
  487.9 225.4 all-gather.21
  728.6 6.3 reduce-scatter.4
where the time goes:
time: 744 us; the launch traced here: 743 us
  waiting for transfers between devices  633 us (85%)
  blocking collectives  45 us (6%)
  matrix products  28.8 us (4%)
  other arithmetic  20.7 us (3%)
  between operations  13.5 us (2%)
    all_gather x1, waiting for transfers between devices, on_device(): lax.all_gather(down_weight.astype(jnp.bfloat16), 'fs', axis=1, tiled=True)  228 us
    all_gather x1, waiting for transfers between devices, on_device(): lax.all_gather(up_weight.astype(jnp.bfloat16), 'fs', axis=0, tiled=True)  207 us
    all_gather x1, waiting for transfers between devices, on_device(): lax.all_gather(out_weight.astype(jnp.bfloat16), 'fs', axis=1, tiled=True)  50.8 us
    all_gather x1, waiting for transfers between devices, on_device(): lax.all_gather(value_weight.astype(jnp.bfloat16), 'fs', axis=0, tiled=True)  46.9 us
    all_gather x1, waiting for transfers between devices, on_device(): lax.all_gather(gate_weight.astype(jnp.bfloat16), 'fs', axis=0, tiled=True)  41.4 us
    all_gather x1, waiting for transfers between devices, on_device(): lax.all_gather(key_weight.astype(jnp.bfloat16), 'fs', axis=0, tiled=True)  39.3 us
    all_gather x1, blocking collectives, on_device(): lax.all_gather(out_scale, 'fs', axis=0, tiled=True)  22.2 us
    dot_general x2, matrix products, column_terms(): lax.dot_general(weight, hidden, (((0,), (1,)), ((), ())), preferred_eleme...  19.4 us
  transfers between devices with their start and end apart: 9, of which 8 were waited for; matrix products, arithmetic and copies ran while one was open for 4% of the time, Pallas kernels for 0%

commit v1 on v0

v1 whole, which is shorter than its diff:
```python
import jax
import jax.numpy as jnp
from jax import lax
from jax.sharding import PartitionSpec as P

BLOCK = 64
LENGTH = 192


epsilon = 1e-06
rope_base = 10000.0


def rotate(head_rows, positions):
    half = head_rows.shape[-1] // 2
    inverse = 1.0 / rope_base ** jnp.linspace(0.0, 1.0, half, dtype=jnp.float32)
    angles = positions[:, None] * inverse[None, :]
    cosine = jnp.cos(angles)[:, None, :]
    sine = jnp.sin(angles)[:, None, :]
    first = head_rows[..., :half]
    second = head_rows[..., half:]
    return jnp.concatenate(
        [first * cosine - second * sine, first * sine + second * cosine], axis=-1
    )


def retain(query_heads, key_heads, value_heads, log_decay):
    batch, length, heads, width = query_heads.shape
    block_count = length // BLOCK
    highest = lax.Precision.HIGHEST

    def to_blocks(tensor):
        return tensor.reshape(batch, block_count, BLOCK, heads, tensor.shape[-1]).transpose(
            0, 3, 1, 2, 4
        )

    query_blocks = to_blocks(query_heads)
    key_blocks = to_blocks(key_heads)
    value_blocks = to_blocks(value_heads)
    places = jnp.arange(BLOCK, dtype=jnp.float32)
    offsets = places[:, None] - places[None, :]
    inner = jnp.where(
        offsets >= 0, jnp.exp(log_decay[:, None, None] * jnp.maximum(offsets, 0.0)), 0.0
    )
    scores = (
        jnp.einsum("bhntd,bhnsd->bhnts", query_blocks, key_blocks, precision=highest)
        * inner[None, :, None]
    )
    output = jnp.einsum("bhnts,bhnse->bhnte", scores, value_blocks, precision=highest)
    keys_decayed = (
        key_blocks
        * jnp.exp(log_decay[:, None] * (BLOCK - 1.0 - places)[None, :])[None, :, None, :, None]
    )
    increments = jnp.einsum("bhnsd,bhnse->nbhde", keys_decayed, value_blocks, precision=highest)
    carry_decay = jnp.exp(log_decay * BLOCK)[None, :, None, None]

    def advance(state, increment):
        return (carry_decay * state + increment, state)

    initial = jnp.zeros((batch, heads, width, value_heads.shape[-1]), jnp.float32)
    _, states = lax.scan(advance, initial, increments)
    query_decayed = (
        query_blocks * jnp.exp(log_decay[:, None] * (places + 1.0)[None, :])[None, :, None, :, None]
    )
    output = output + jnp.einsum("bhntd,nbhde->bhnte", query_decayed, states, precision=highest)
    return output.transpose(0, 2, 3, 1, 4).reshape(batch, length, heads, value_heads.shape[-1])


def norm_half(rows, gain):
    wide = rows.astype(jnp.float32)
    total = lax.psum(jnp.sum(wide * wide, axis=1, keepdims=True), "tp")
    width = rows.shape[1]
    parts = lax.axis_size("tp")
    mine = lax.dynamic_slice(gain, (lax.axis_index("tp") * width,), (width,))
    scaled = wide * lax.rsqrt(total / (width * parts) + epsilon) * mine
    return scaled.astype(jnp.bfloat16)


def tp_columns(rows):
    return lax.all_gather(rows, "tp", axis=1, tiled=True)


def heads_of(normed, weight, scale):
    return jnp.dot(normed, weight, preferred_element_type=jnp.float32) * scale


def mixer(activations, mix_gain, four, four_scale, out_full, out_columns, log_decay):
    normed = tp_columns(norm_half(activations, mix_gain))
    total_rows = normed.shape[0]
    sequences = total_rows // LENGTH
    heads = log_decay.shape[0]
    joined = heads_of(normed, four, four_scale)
    unit = joined.shape[1] // 6
    query = joined[:, :unit]
    key_rows = joined[:, unit : 2 * unit]
    value = joined[:, 2 * unit : 4 * unit]
    gate = joined[:, 4 * unit :]
    positions = jnp.arange(LENGTH, dtype=jnp.float32)
    query_heads = rotate(query.reshape(sequences, LENGTH, heads, -1), positions)
    key_heads = rotate(key_rows.reshape(sequences, LENGTH, heads, -1), positions)
    value_heads = value.reshape(sequences, LENGTH, heads, -1)
    retained = retain(query_heads, key_heads, value_heads, log_decay)
    retained = retained * lax.rsqrt(jnp.mean(retained * retained, axis=-1, keepdims=True) + epsilon)
    attended = (retained.reshape(total_rows, -1) * jax.nn.silu(gate)).astype(jnp.bfloat16)
    partial_value = jnp.einsum(
        "rk,jkc->rjc", attended, out_full, preferred_element_type=jnp.float32
    ).reshape(total_rows, -1)
    partial_value = (partial_value * out_columns).astype(jnp.bfloat16)
    mixed = tp_sum(partial_value)
    return (activations.astype(jnp.float32) + mixed).astype(jnp.bfloat16)


def tp_sum(partial_value):
    parts = lax.axis_size("tp")
    width = partial_value.shape[1] // parts
    spread = jnp.moveaxis(partial_value.reshape(-1, parts, width), 1, 0)
    arrived = lax.all_to_all(spread, "tp", 0, 0, tiled=True)
    return jnp.sum(arrived.astype(jnp.float32), axis=0)


def on_device(
    activations,
    mix_gain,
    mlp_gain,
    query_weight,
    query_scale,
    key_weight,
    key_scale,
    value_weight,
    value_scale,
    gate_weight,
    gate_scale,
    out_weight,
    out_scale,
    up_weight,
    up_scale,
    down_weight,
    down_scale,
    log_decay,
):
    bf = jnp.bfloat16
    four_weight = jnp.concatenate(
        [query_weight, key_weight, value_weight, gate_weight], axis=1
    ).astype(bf)
    four_scale = jnp.concatenate([query_scale, key_scale, value_scale, gate_scale])
    four = lax.all_gather(four_weight, "fs", axis=0, tiled=True)
    out_full = lax.all_gather(out_weight.astype(bf), "fs", axis=0)
    scales = lax.all_gather(jnp.stack([out_scale, down_scale]), "fs", axis=1, tiled=True)
    up_mine = lax.all_to_all(up_weight.astype(bf), "fs", 1, 0, tiled=True)
    down_mine = lax.all_to_all(down_weight.astype(bf), "fs", 0, 1, tiled=True)
    units = up_mine.shape[1]
    up_columns = lax.dynamic_slice(up_scale, (lax.axis_index("fs") * units,), (units,))
    first = mixer(activations, mix_gain, four, four_scale, out_full, scales[0], log_decay)
    half_rows = norm_half(first, mlp_gain)
    normed_two = tp_columns(lax.all_gather(half_rows, "fs", axis=0, tiled=True))
    raised = jnp.dot(normed_two, up_mine, preferred_element_type=jnp.float32) * up_columns
    hidden = jnp.square(jax.nn.relu(raised)).astype(bf)
    share = jnp.dot(hidden, down_mine, preferred_element_type=jnp.float32) * scales[1]
    pair = tp_sum(share.astype(bf)).astype(bf)
    arrived = lax.all_to_all(
        pair.reshape(-1, first.shape[0], first.shape[1]), "fs", 0, 0, tiled=True
    )
    channel = jnp.sum(arrived.astype(jnp.float32), axis=0)
    return (first.astype(jnp.float32) + channel).astype(bf)


def solution(mesh):
    placed = (
        P(("rep", "fs"), "tp"),
        P(),
        P(),
        P("fs", "tp"),
        P("tp"),
        P("fs", "tp"),
        P("tp"),
        P("fs", "tp"),
        P("tp"),
        P("fs", "tp"),
        P("tp"),
        P("tp", "fs"),
        P("fs"),
        P("fs", "tp"),
        P("tp"),
        P("tp", "fs"),
        P("fs"),
        P("tp"),
    )
    return jax.shard_map(
        on_device, mesh=mesh, in_specs=placed, out_specs=P(("rep", "fs"), "tp"), check_vma=False
    )
```

time: 744 us -> 447 us (0.60)
  waiting for transfers between devices: 633 us -> 238 us
  blocking collectives: 45 us -> 125 us
  local copies, waits for them, and re-layouts: 2.06 us -> 19.9 us
  matrix products: 28.8 us -> 20.5 us
  starting transfers between devices: 0.34 us -> 8.33 us
    all_gather x7 -> x4, waiting for transfers between devices: 626 us -> 193 us  [the longest x1 87.2 us: on_device(): normed_two = tp_columns(lax.all_gather(half_rows, 'fs', axis=0, tiled=True))]
    all_to_all x0 -> x3, blocking collectives: none -> 88.7 us  [the longest x1 74.4 us: on_device(): lax.all_to_all(pair.reshape(-1, first.shape[0], first.shape[1]), 'fs', 0,...]
    all_to_all x0 -> x2, waiting for transfers between devices: none -> 44.7 us  [the longest x1 44.7 us: on_device(): down_mine = lax.all_to_all(down_weight.astype(bf), 'fs', 0, 1, tiled=True)]
    all_gather x4 -> x2, blocking collectives: 45 us -> 31 us  [the longest x1 28.7 us: on_device(): lax.all_gather(jnp.stack([out_scale, down_scale]), 'fs', axis=1, tiled=True)]
    convert_element_type x9 -> x5, other arithmetic: 17.3 us -> 6.48 us  [the longest x1 3.84 us: on_device(): down_mine = lax.all_to_all(down_weight.astype(bf), 'fs', 0, 1, tiled=True)]
    all_to_all x0 -> x2, starting transfers between devices: none -> 8.2 us  [the longest x1 4.6 us: on_device(): down_mine = lax.all_to_all(down_weight.astype(bf), 'fs', 0, 1, tiled=True)]
    dot_general x5 -> x3, matrix products: 24.9 us -> 17.6 us  [the longest x1 11.1 us: on_device(): jnp.dot(hidden, down_mine, preferred_element_type=jnp.float32) * scales[1]]
  transfers between devices with their start and end apart: 9 -> 6, of which waited for: 8 -> 4; matrix products, arithmetic and copies ran while one was open for 4% -> 6% of each run, Pallas kernels for 0% -> 0%
where the time goes in v1:
time: 447 us; the launch traced here: 446 us
  waiting for transfers between devices  238 us (53%)
  blocking collectives  125 us (28%)
  other arithmetic  20.5 us (5%)
  matrix products  20.5 us (5%)
  local copies, waits for them, and re-layouts  19.9 us (4%)
  between operations  13.6 us (3%)
  starting transfers between devices  8.33 us (2%)
    all_gather x1, waiting for transfers between devices, on_device(): normed_two = tp_columns(lax.all_gather(half_rows, 'fs', axis=0, tiled=True))  87.2 us
    all_to_all x1, blocking collectives, on_device(): lax.all_to_all(pair.reshape(-1, first.shape[0], first.shape[1]), 'fs', 0,...  74.4 us
    all_gather x1, waiting for transfers between devices, on_device(): four = lax.all_gather(four_weight, 'fs', axis=0, tiled=True)  66.2 us
    all_to_all x1, waiting for transfers between devices, on_device(): down_mine = lax.all_to_all(down_weight.astype(bf), 'fs', 0, 1, tiled=True)  44.7 us
    all_gather x1, waiting for transfers between devices, on_device(): out_full = lax.all_gather(out_weight.astype(bf), 'fs', axis=0)  40.1 us
    all_gather x1, blocking collectives, on_device(): lax.all_gather(jnp.stack([out_scale, down_scale]), 'fs', axis=1, tiled=True)  28.7 us
    all_to_all x2, blocking collectives, tp_sum(): arrived = lax.all_to_all(spread, 'tp', 0, 0, tiled=True)  14.3 us
    dot_general x1, matrix products, on_device(): jnp.dot(hidden, down_mine, preferred_element_type=jnp.float32) * scales[1]  11.1 us
  transfers between devices with their start and end apart: 6, of which 4 were waited for; matrix products, arithmetic and copies ran while one was open for 6% of the time, Pallas kernels for 0%

profile of v1, /device:TPU:0, one launch (start us, length us, event | category | flops | bytes accessed | tf_op | source)
XLA Modules:
  0.0 445.8 jit_solution(648418608452168935)
XLA Ops:
  6.5 1.0 convert.13
  7.5 1.0 convert.14
  8.5 1.1 convert.15
  9.6 1.1 convert.16
  10.8 1.0 pad_maximum_fusion
  13.1 2.6 psum.14
  15.7 28.7 %all_gather.25 = f32[2,2048]{1,0:T(2,128)S(1)} all-gather(f32[2,256]{1,0:T(2,128)S(1)} %pad_maximum_fusion.4), channel_id=1, replica_groups=mesh['rep'=2,'fs'=8,'tp'=2] {'fs'}, dimensions={1}, use_global_device_ids=true | all-gather | bytes 18432 | tf_op jit(solution)/shard_map/all_gather | solution.py:148
  45.0 2.4 all_gather.21
  47.5 66.2 %all-gather.6.cloned.1.call-done = bf16[2048,1536]{1,0:T(8,128)(2,1)} async-done(((bf16[256,1536]{1,0:T(8,128)(2,1)}), bf16[2048,1536]{1,0:T(8,128)(2,1)}) %all-gather.6.cloned.1.call-update) | async-done | bytes 6291472 | tf_op jit(solution)/shard_map/all_gather | solution.py:146
  113.6 4.2 convolution_multiply_fusion.1
  119.3 0.9 convolution_bitcast_fusion
  123.0 40.1 %all-gather.12.cloned.1.call-done = bf16[4096,256]{1,0:T(8,128)(2,1)} async-done(((bf16[512,256]{1,0:T(8,128)(2,1)}), bf16[4096,256]{1,0:T(8,128)(2,1)}) %all-gather.12.cloned.1.call-update) | async-done | bytes 2097168 | tf_op jit(solution)/shard_map/all_gather | solution.py:147
  163.3 2.3 fusion.24
  165.7 0.9 copy.95
  166.6 1.0 reshape.249
  168.4 4.4 all_to_all.53
  173.1 2.5 psum.15
  175.6 0.9 fusion.10
  176.5 4.6 %copy.97 = bf16[256,4096]{0,1:T(8,128)(2,1)} copy(f32[256,4096]{1,0:T(8,128)} %param.35) | data formatting | bytes 6291456 | tf_op args[13]
  181.1 3.6 all-to-all-start.1
  184.8 87.2 %all-gather.8.cloned.1.call-done = bf16[1536,1024]{1,0:T(8,128)(2,1)} async-done(((bf16[192,1024]{1,0:T(8,128)(2,1)}), bf16[1536,1024]{1,0:T(8,128)(2,1)}) %all-gather.8.cloned.1.call-update) | async-done | bytes 3145744 | tf_op jit(solution)/shard_map/all_gather | solution.py:155
  272.1 3.8 convert_element_type.62
  275.9 4.6 %all-to-all-start.2 = ((bf16[8,512,256]{2,1,0:T(8,128)(2,1)}), bf16[8,512,256]{2,1,0:T(8,128)(2,1)}, u32[]{:S(2)}, u32[]{:S(2)}) async-start(bf16[8,512,256]{2,1,0:T(8,128)(2,1)} %bitcast.37), calls=%async_computation.2 | async-start | bytes 4194304 | tf_op jit(solution)/shard_map/all_to_all | solution.py:150
  281.3 2.4 copy.98
  283.7 44.7 %all-to-all-done.2 = bf16[8,512,256]{2,1,0:T(8,128)(2,1)} async-done(((bf16[8,512,256]{2,1,0:T(8,128)(2,1)}), bf16[8,512,256]{2,1,0:T(8,128)(2,1)}, u32[]{:S(2)}, u32[]{:S(2)}) %all-to-all-start.2) | async-done | bytes 2097184 | tf_op jit(solution)/shard_map/all_to_all | solution.py:150
  328.3 4.1 copy.99
  332.4 11.1 %multiply_convert_fusion = bf16[1536,2048]{1,0:T(8,128)(2,1)} fusion(bf16[512,2048]{0,1:T(8,128)(2,1)} %bitcast.119, f32[2048]{0:T(1024)S(1)} %bitcast.126, bf16[1536,2048]{1,0:T(8,128)(2,1)} %all-gather.10.cloned.1.call-done, bf16[2048,512]{1,0:T(8,128)(2,1)S(1)} %bitcast.118, f32[512]{0:T(512)S(1)} %dynamic_slice.15), kind=kOutput, calls=%fused_computation.2 | convolution fusion | flops 6451888128 | bytes 16787456 | tf_op jit(solution)/shard_map/dot_general | solution.py:158
  343.5 3.5 copy.131
  347.0 10.0 %all_to_all.54 = bf16[2,1536,1024]{2,1,0:T(8,128)(2,1)} all-to-all(bf16[2,1536,1024]{2,1,0:T(8,128)(2,1)S(1)} %bitcast.109), channel_id=1, replica_groups=mesh['rep'=2,'fs'=8,'tp'=2] {'tp'}, dimensions={0} | all-to-all | bytes 12582912 | tf_op jit(solution)/shard_map/all_to_all | solution.py:117
  356.9 6.2 %reduce_sum.61 = bf16[1536,1024]{1,0:T(8,128)(2,1)S(1)} reduce(bf16[2,1536,1024]{2,1,0:T(8,128)(2,1)} %all_to_all.54, bf16[]{:T(256)} %constant.62.clone.1), dimensions={0}, to_apply=%region_8.10 | reduce | flops 1572864 | bytes 9437186 | tf_op jit(solution)/shard_map/reduce_sum | solution.py:118
  363.1 74.4 %all_to_all.55 = bf16[8,192,1024]{2,1,0:T(8,128)(2,1)S(1)} all-to-all(bf16[8,192,1024]{2,1,0:T(8,128)(2,1)S(1)} %bitcast.110), channel_id=1, replica_groups=mesh['rep'=2,'fs'=8,'tp'=2] {'fs'}, dimensions={0} | all-to-all | bytes 6291456 | tf_op jit(solution)/shard_map/all_to_all | solution.py:160
  438.5 0.8 fusion.11
  (92 shorter events, 9.5 us)
Async XLA Ops:
  6.5 107.1 %all-gather.6.cloned.1.call-start = ((), (), s32[]{:S(2)}) async-start(), calls=%async_computation.5 | async-start | bytes 7077888 | tf_op jit(solution)/shard_map/all_gather | solution.py:146
  7.5 4.5 copy-start.5
  9.6 3.2 copy-start.7
  9.6 3.3 copy-start
  10.8 4.9 %copy-start.13 = (f32[256]{0:T(256)S(1)}, f32[256]{0:T(256)}, u32[]{:S(2)}) copy-start(f32[256]{0:T(256)} %param.38) | copy-start | bytes 3076
  10.8 4.9 %copy-start.14 = (f32[256]{0:T(256)S(1)}, f32[256]{0:T(256)}, u32[]{:S(2)}) copy-start(f32[256]{0:T(256)} %param.34) | copy-start | bytes 3076
  10.8 34.0 %copy-start.10 = (f32[2048]{0:T(1024)S(1)}, f32[2048]{0:T(1024)}, u32[]{:S(2)}) copy-start(f32[2048]{0:T(1024)} %param.23) | copy-start | bytes 24580
  11.9 35.6 %copy-start.8 = (f32[512]{0:T(512)S(1)}, f32[512]{0:T(512)}, u32[]{:S(2)}) copy-start(f32[512]{0:T(512)} %param.32) | copy-start | bytes 6148
  11.9 35.6 %copy-start.9 = (f32[512]{0:T(512)S(1)}, f32[512]{0:T(512)}, u32[]{:S(2)}) copy-start(f32[512]{0:T(512)} %param.30) | copy-start | bytes 6148
  11.9 35.6 %copy-start.11 = (f32[256]{0:T(256)S(1)}, f32[256]{0:T(256)}, u32[]{:S(2)}) copy-start(f32[256]{0:T(256)} %param.28) | copy-start | bytes 3076
  11.9 35.6 %copy-start.12 = (f32[256]{0:T(256)S(1)}, f32[256]{0:T(256)}, u32[]{:S(2)}) copy-start(f32[256]{0:T(256)} %param.26) | copy-start | bytes 3076
  11.9 151.1 %all-gather.12.cloned.1.call-start = ((), (), s32[]{:S(2)}) async-start(), calls=%async_computation.8 | async-start | bytes 2359296 | tf_op jit(solution)/shard_map/all_gather | solution.py:147
  12.7 259.3 %all-gather.8.cloned.1.call-start = ((), (), s32[]{:S(2)}) async-start(), calls=%async_computation.6 | async-start | bytes 3538944 | tf_op jit(solution)/shard_map/all_gather | solution.py:155
  117.8 1.0 copy-start.4
  119.1 2.4 copy-start.6
  168.4 7.2 %dynamic-slice-start = ((f32[2048]{0:T(1024)}, s32[]{:T(128)}), f32[1024]{0:T(1024)S(1)}, s32[]{:S(2)}) async-start(f32[2048]{0:T(1024)} %param.24, s32[]{:T(128)} %select_n.15), calls=%async_computation.9 | async-start | bytes 8704 | tf_op jit(solution)/shard_map/dynamic_slice | solution.py:74
  173.1 8.1 %copy-start.1 = (bf16[192,1024]{1,0:T(8,128)(2,1)}, bf16[192,1024]{1,0:T(8,128)(2,1)S(1)}, u32[]{:S(2)}) copy-start(bf16[192,1024]{1,0:T(8,128)(2,1)S(1)} %get-tuple-element.93) | copy-start | bytes 1179652
  181.1 94.8 %all-to-all-start.1 = ((bf16[256,8,512]{0,2,1:T(8,128)(2,1)}), bf16[256,8,512]{0,2,1:T(8,128)(2,1)S(1)}, u32[]{:S(2)}, u32[]{:S(2)}) async-start(bf16[256,8,512]{0,2,1:T(8,128)(2,1)} %bitcast.34), calls=%async_computation.1 | async-start | bytes 4194304 | tf_op jit(solution)/shard_map/all_to_all | solution.py:149
  184.8 147.6 %all-gather.10.cloned.1.call-start = ((), (), s32[]{:S(2)}) async-start(), calls=%async_computation.7 | async-start | bytes 9437184 | tf_op jit(solution)/shard_map/all_gather | solution.py:80
  275.9 52.4 %all-to-all-start.2 = ((bf16[8,512,256]{2,1,0:T(8,128)(2,1)}), bf16[8,512,256]{2,1,0:T(8,128)(2,1)}, u32[]{:S(2)}, u32[]{:S(2)}) async-start(bf16[8,512,256]{2,1,0:T(8,128)(2,1)} %bitcast.37), calls=%async_computation.2 | async-start | bytes 4194304 | tf_op jit(solution)/shard_map/all_to_all | solution.py:150
  328.3 4.1 copy-start.3
  437.5 1.0 copy-start.2
Sparse Core Ops, SparseCore 0:
  12.0 101.6 all-gather.5
  115.8 47.2 all-gather.11
  176.6 95.3 all-gather.7
  273.4 14.1 all-gather.9

commit v2 on v1

--- a/solution.py
+++ b/solution.py
@@ -1,6 +1,10 @@
+import functools
+
 import jax
 import jax.numpy as jnp
 from jax import lax
+from jax.experimental import pallas as pl
+from jax.experimental.pallas import tpu as pltpu
 from jax.sharding import PartitionSpec as P
 
 BLOCK = 64
@@ -64,6 +68,294 @@
     )
     output = output + jnp.einsum("bhntd,nbhde->bhnte", query_decayed, states, precision=highest)
     return output.transpose(0, 2, 3, 1, 4).reshape(batch, length, heads, value_heads.shape[-1])
+
+
+MESH = pl.DeviceIdType.MESH
+
+
+def ring_place(index, n):
+    odd = index % 2
+    return (1 - odd) * (index // 2) + odd * (n - 1 - index // 2)
+
+
+def ring_index(place, n):
+    place = (place + n) % n
+    late = (2 * place) // n
+    return (1 - late) * (2 * place) + late * (2 * (n - 1 - place) + 1)
+
+
+def greet(targets):
+    barrier = pltpu.get_barrier_semaphore()
+    for target in targets:
+        pl.semaphore_signal(barrier, inc=1, device_id=target, device_id_type=MESH)
+    pl.semaphore_wait(barrier, len(targets))
+
+
+def remote(source, target, send, recv, device):
+    return pltpu.make_async_remote_copy(
+        src_ref=source,
+        dst_ref=target,
+        send_sem=send,
+        recv_sem=recv,
+        device_id=device,
+        device_id_type=MESH,
+    )
+
+
+def ring_gather_kernel(n, count, shared, *refs):
+    ins, outs = refs[:count], refs[count : 2 * count]
+    own_sem, send_sem, recv_sem, xsend_sem, xrecv_sem = refs[2 * count :]
+    me = lax.axis_index("fs")
+    place = ring_place(me, n)
+    chunks = ins[0].shape[0]
+    quarter = chunks // 4
+    right = {"fs": ring_index(place + 1, n)}
+    left = {"fs": ring_index(place + n - 1, n)}
+    targets = [right, left]
+    if shared:
+        rep = lax.axis_index("rep")
+        across = {"rep": 1 - rep}
+        targets.append(across)
+        lanes = [
+            (rep * 2, 1, 0),
+            (rep * 2 + 1, -1, 1),
+            (4, 1, None),
+            (6, -1, None),
+            (5, 1, None),
+            (7, -1, None),
+        ]
+    else:
+        lanes = [(k, 1 if k % 2 == 0 else -1, None) for k in range(chunks)]
+    greet(targets)
+    owns = [
+        pltpu.make_async_copy(ins[a], outs[a].at[me], own_sem.at[a]) for a in range(count)
+    ]
+    for own in owns:
+        own.start()
+    for k, (chunk, way, _) in enumerate(lanes):
+        for a in range(count):
+            remote(
+                ins[a].at[chunk],
+                outs[a].at[me, chunk],
+                send_sem.at[a, k],
+                recv_sem.at[0, a, k],
+                right if way == 1 else left,
+            ).start()
+
+    def step(s, _):
+        for k, (chunk, way, extra) in enumerate(lanes):
+            owner = ring_index(place + (n - s if way == 1 else s), n)
+            for a in range(count):
+                block = outs[a].at[owner, chunk]
+                device = right if way == 1 else left
+                remote(block, block, send_sem.at[a, k], recv_sem.at[s - 1, a, k], device).wait()
+
+                @pl.when(s < n - 1)
+                def _():
+                    remote(
+                        block, block, send_sem.at[a, k], recv_sem.at[s, a, k], device
+                    ).start()
+
+                if extra is not None:
+
+                    @pl.when(s > 1)
+                    def _():
+                        remote(
+                            block,
+                            block,
+                            xsend_sem.at[a, extra],
+                            xrecv_sem.at[s - 1, a, extra],
+                            across,
+                        ).wait_send()
+
+                    remote(
+                        block,
+                        block,
+                        xsend_sem.at[a, extra],
+                        xrecv_sem.at[s - 1, a, extra],
+                        across,
+                    ).start()
+        return 0
+
+    lax.fori_loop(1, n, step, 0)
+    if shared:
+        for a in range(count):
+            for extra in range(2):
+                block = outs[a].at[me, extra]
+                remote(
+                    block, block, xsend_sem.at[a, extra], xrecv_sem.at[0, a, extra], across
+                ).wait_send()
+
+        def close(s, _):
+            for a in range(count):
+                for extra in range(2):
+                    way = 1 if extra == 0 else -1
+                    owner = ring_index(place + (n - s if way == 1 else s), n)
+                    block = outs[a].at[owner, (1 - rep) * 2 + extra]
+                    remote(
+                        block,
+                        block,
+                        xsend_sem.at[a, extra],
+                        xrecv_sem.at[s - 1, a, extra],
+                        across,
+                    ).wait_recv()
+            return 0
+
+        lax.fori_loop(1, n, close, 0)
+    for own in owns:
+        own.wait()
+
+
+def ring_gather(arrays, n, shared, identity):
+    count = len(arrays)
+    lanes = 6 if shared else arrays[0].shape[0]
+    dma = pltpu.SemaphoreType.DMA
+    return pl.pallas_call(
+        functools.partial(ring_gather_kernel, n, count, shared),
+        out_shape=[jax.ShapeDtypeStruct((n,) + a.shape, a.dtype) for a in arrays],
+        in_specs=[pl.BlockSpec(memory_space=pltpu.VMEM)] * count,
+        out_specs=[pl.BlockSpec(memory_space=pl.ANY)] * count,
+        scratch_shapes=[
+            dma((count,)),
+            dma((count, lanes)),
+            dma((n - 1, count, lanes)),
+            dma((count, 2)),
+            dma((n - 1, count, 2)),
+        ],
+        compiler_params=pltpu.CompilerParams(collective_id=identity, has_side_effects=True),
+    )(*arrays)
+
+
+def spread_kernel(n, count, *refs):
+    ins, outs = refs[:count], refs[count : 2 * count]
+    own_sem, send_sem, recv_sem, xsend_sem, xrecv_sem = refs[2 * count :]
+    me = lax.axis_index("fs")
+    rep = lax.axis_index("rep")
+    across = {"rep": 1 - rep}
+    greet([{"fs": (me + d) % n} for d in range(1, n)] + [across])
+    owns = [
+        pltpu.make_async_copy(ins[a].at[me], outs[a].at[me], own_sem.at[a]) for a in range(count)
+    ]
+    for own in owns:
+        own.start()
+
+    def sending(d, a):
+        peer = (me + d) % n
+        return remote(
+            ins[a].at[peer, rep],
+            outs[a].at[me, rep],
+            send_sem.at[a, d - 1],
+            recv_sem.at[a, d - 1],
+            {"fs": peer},
+        )
+
+    def crossing(d, a, half):
+        block = outs[a].at[(me + n - d) % n, half]
+        return remote(block, block, xsend_sem.at[a, d - 1], xrecv_sem.at[a, d - 1], across)
+
+    def begin(d, _):
+        for a in range(count):
+            sending(d, a).start()
+        return 0
+
+    def relay(d, _):
+        for a in range(count):
+            block = outs[a].at[(me + n - d) % n, rep]
+            remote(
+                block,
+                block,
+                send_sem.at[a, d - 1],
+                recv_sem.at[a, d - 1],
+                {"fs": (me + d) % n},
+            ).wait_recv()
+            crossing(d, a, rep).start()
+        return 0
+
+    def close(d, _):
+        for a in range(count):
+            sending(d, a).wait_send()
+            crossing(d, a, rep).wait_send()
+            crossing(d, a, 1 - rep).wait_recv()
+        return 0
+
+    lax.fori_loop(1, n, begin, 0)
+    lax.fori_loop(1, n, relay, 0)
+    lax.fori_loop(1, n, close, 0)
+    for own in owns:
+        own.wait()
+
+
+def spread(arrays, n, identity):
+    count = len(arrays)
+    dma = pltpu.SemaphoreType.DMA
+    return pl.pallas_call(
+        functools.partial(spread_kernel, n, count),
+        out_shape=[jax.ShapeDtypeStruct(a.shape, a.dtype) for a in arrays],
+        in_specs=[pl.BlockSpec(memory_space=pltpu.VMEM)] * count,
+        out_specs=[pl.BlockSpec(memory_space=pl.ANY)] * count,
+        scratch_shapes=[dma((count,))] + [dma((count, n - 1)) for _ in range(4)],
+        compiler_params=pltpu.CompilerParams(collective_id=identity, has_side_effects=True),
+    )(*arrays)
+
+
+def ring_sum_kernel(n, in_ref, out_ref, held, send_sem, recv_sem):
+    me = lax.axis_index("fs")
+    place = ring_place(me, n)
+    right = {"fs": ring_index(place + 1, n)}
+    left = {"fs": ring_index(place + n - 1, n)}
+    greet([right, left])
+    pieces = in_ref.shape[1]
+
+    def hop(s, k, source):
+        return remote(
+            source,
+            held.at[s, k],
+            send_sem.at[s, k],
+            recv_sem.at[s, k],
+            right if k % 2 == 0 else left,
+        )
+
+    def owner(s, k):
+        return ring_index(place + (2 * n - 1 - s if k % 2 == 0 else 1 + s), n)
+
+    for k in range(pieces):
+        hop(0, k, in_ref.at[owner(0, k), k]).start()
+
+    def step(s, _):
+        for k in range(pieces):
+            hop(s - 1, k, held.at[s - 1, k]).wait_recv()
+            total = held[s - 1, k].astype(jnp.float32) + in_ref[owner(s, k), k].astype(jnp.float32)
+            held[s - 1, k] = total.astype(jnp.bfloat16)
+            hop(s, k, held.at[s - 1, k]).start()
+        return 0
+
+    lax.fori_loop(1, n - 1, step, 0)
+    for k in range(pieces):
+        hop(n - 2, k, held.at[n - 2, k]).wait_recv()
+        out_ref[k] = held[n - 2, k].astype(jnp.float32) + in_ref[me, k].astype(jnp.float32)
+
+    def close(s, _):
+        for k in range(pieces):
+            hop(s, k, held.at[s, k]).wait_send()
+        return 0
+
+    lax.fori_loop(0, n - 1, close, 0)
+
+
+def ring_sum(shares, n, identity):
+    dma = pltpu.SemaphoreType.DMA
+    return pl.pallas_call(
+        functools.partial(ring_sum_kernel, n),
+        out_shape=jax.ShapeDtypeStruct(shares.shape[1:], jnp.float32),
+        in_specs=[pl.BlockSpec(memory_space=pltpu.VMEM)],
+        out_specs=pl.BlockSpec(memory_space=pltpu.VMEM),
+        scratch_shapes=[
+            pltpu.VMEM((n - 1,) + shares.shape[1:], shares.dtype),
+            dma((n - 1, shares.shape[1])),
+            dma((n - 1, shares.shape[1])),
+        ],
+        compiler_params=pltpu.CompilerParams(collective_id=identity, has_side_effects=True),
+    )(shares)
 
 
 def norm_half(rows, gain):
@@ -143,24 +435,46 @@
         [query_weight, key_weight, value_weight, gate_weight], axis=1
     ).astype(bf)
     four_scale = jnp.concatenate([query_scale, key_scale, value_scale, gate_scale])
-    four = lax.all_gather(four_weight, "fs", axis=0, tiled=True)
-    out_full = lax.all_gather(out_weight.astype(bf), "fs", axis=0)
-    scales = lax.all_gather(jnp.stack([out_scale, down_scale]), "fs", axis=1, tiled=True)
-    up_mine = lax.all_to_all(up_weight.astype(bf), "fs", 1, 0, tiled=True)
-    down_mine = lax.all_to_all(down_weight.astype(bf), "fs", 0, 1, tiled=True)
+    n = lax.axis_size("fs")
+    out_half = out_weight.astype(bf)
+    spare = jnp.stack([out_scale, down_scale])
+    four, out_full, scales = ring_gather(
+        [
+            four_weight.reshape(8, -1, four_weight.shape[1]),
+            out_half.reshape(8, -1, out_half.shape[1]),
+            jnp.broadcast_to(spare, (8,) + spare.shape),
+        ],
+        n,
+        True,
+        0,
+    )
+    four = four.reshape(-1, four_weight.shape[1])
+    out_full = out_full.reshape((n,) + out_half.shape)
+    scales = jnp.moveaxis(scales[:, 0], 1, 0).reshape(2, -1)
+    depth = up_weight.shape[0]
+    up_cut = jnp.moveaxis(up_weight.astype(bf).reshape(depth, n, -1), 1, 0)
+    down_cut = down_weight.astype(bf).reshape(n, 2, -1, down_weight.shape[1])
+    up_mine, down_mine = spread(
+        [up_cut.reshape(n, 2, depth // 2, -1), down_cut], n, 1
+    )
+    up_mine = up_mine.reshape(n * depth, -1)
+    down_mine = down_mine.reshape(n, -1, down_weight.shape[1])
     units = up_mine.shape[1]
     up_columns = lax.dynamic_slice(up_scale, (lax.axis_index("fs") * units,), (units,))
     first = mixer(activations, mix_gain, four, four_scale, out_full, scales[0], log_decay)
     half_rows = norm_half(first, mlp_gain)
-    normed_two = tp_columns(lax.all_gather(half_rows, "fs", axis=0, tiled=True))
+    normed_two = tp_columns(
+        ring_gather([half_rows.reshape(4, -1, half_rows.shape[1])], n, False, 2)[0].reshape(
+            -1, half_rows.shape[1]
+        )
+    )
     raised = jnp.dot(normed_two, up_mine, preferred_element_type=jnp.float32) * up_columns
     hidden = jnp.square(jax.nn.relu(raised)).astype(bf)
-    share = jnp.dot(hidden, down_mine, preferred_element_type=jnp.float32) * scales[1]
+    share = jnp.einsum("ru,jud->rjd", hidden, down_mine, preferred_element_type=jnp.float32)
+    share = share.reshape(share.shape[0], -1) * scales[1]
     pair = tp_sum(share.astype(bf)).astype(bf)
-    arrived = lax.all_to_all(
-        pair.reshape(-1, first.shape[0], first.shape[1]), "fs", 0, 0, tiled=True
-    )
-    channel = jnp.sum(arrived.astype(jnp.float32), axis=0)
+    shares = pair.reshape(n, 4, -1, first.shape[1])
+    channel = ring_sum(shares, n, 3).reshape(first.shape)
     return (first.astype(jnp.float32) + channel).astype(bf)
 
 

time: 447 us -> 309 us (0.69)
  waiting for transfers between devices: 238 us -> 1.88 us
  Pallas kernels: 0 us -> 208 us
  blocking collectives: 125 us -> 17.8 us
  starting transfers between devices: 8.33 us -> 3.71 us
    pallas_call x0 -> x4, Pallas kernels: none -> 208 us  [the longest x2 107 us: ring_gather(): pl.pallas_call(functools.partial(ring_gather_kernel, n, count, shared), o...]
    all_gather x3 -> x0, waiting for transfers between devices: 193 us -> none  [the longest x1 87.2 us: on_device(): normed_two = tp_columns(lax.all_gather(half_rows, 'fs', axis=0, tiled=True))]
    all_to_all x1 -> x0, blocking collectives: 74.4 us -> none  [on_device(): lax.all_to_all(pair.reshape(-1, first.shape[0], first.shape[1]), 'fs', 0,...]
    all_to_all x2 -> x1, waiting for transfers between devices: 44.7 us -> 1.87 us  [tp_sum(): arrived = lax.all_to_all(spread, 'tp', 0, 0, tiled=True)]
    all_gather x1 -> x0, blocking collectives: 28.7 us -> none  [on_device(): lax.all_gather(jnp.stack([out_scale, down_scale]), 'fs', axis=1, tiled=True)]
    all_to_all x2 -> x0, local copies, waits for them, and re-layouts: 6.44 us -> none  [the longest x1 4.06 us: on_device(): down_mine = lax.all_to_all(down_weight.astype(bf), 'fs', 0, 1, tiled=True)]
    reshape x1 -> x3, local copies, waits for them, and re-layouts: 1.01 us -> 6.92 us  [the longest x1 2.87 us: on_device(): down_mine = down_mine.reshape(n, -1, down_weight.shape[1])]
    all_to_all x2 -> x1, starting transfers between devices: 8.2 us -> 3.67 us  [tp_sum(): arrived = lax.all_to_all(spread, 'tp', 0, 0, tiled=True)]
  transfers between devices with their start and end apart: 6 -> 2, of which waited for: 4 -> 1; matrix products, arithmetic and copies ran while one was open for 6% -> 3% of each run, Pallas kernels for 0% -> 18%
where the time goes in v2:
time: 309 us; the launch traced here: 308 us
  Pallas kernels  208 us (67%)
  other arithmetic  23.3 us (8%)
  matrix products  22.1 us (7%)
  blocking collectives  17.8 us (6%)
  local copies, waits for them, and re-layouts  17.7 us (6%)
  between operations  13.8 us (4%)
  starting transfers between devices  3.71 us (1%)
    pallas_call x2, Pallas kernels, ring_gather(): pl.pallas_call(functools.partial(ring_gather_kernel, n, count, shared), o...  107 us
    pallas_call x1, Pallas kernels, spread(): pl.pallas_call(functools.partial(spread_kernel, n, count), out_shape=[jax...  55.3 us
    pallas_call x1, Pallas kernels, ring_sum(): pl.pallas_call(functools.partial(ring_sum_kernel, n), out_shape=jax.Shape...  45.8 us
    dot_general x1, matrix products, on_device(): jnp.einsum('ru,jud->rjd', hidden, down_mine, preferred_element_type=jnp.f...  11 us
    all_to_all x1, blocking collectives, tp_sum(): arrived = lax.all_to_all(spread, 'tp', 0, 0, tiled=True)  9.99 us
    reduce_sum x2, other arithmetic, tp_sum(): return jnp.sum(arrived.astype(jnp.float32), axis=0)  7.21 us
  transfers between devices with their start and end apart: 2, of which 1 were waited for; matrix products, arithmetic and copies ran while one was open for 3% of the time, Pallas kernels for 18%

profile of v2, /device:TPU:0, one launch (start us, length us, event | category | flops | bytes accessed | tf_op | source)
XLA Modules:
  0.0 308.3 jit_solution(13089728123120259235)
XLA Ops:
  6.6 1.2 fusion.5
  7.9 2.6 psum.14
  10.5 1.0 convert.17
  11.5 1.0 convert.18
  12.5 1.1 convert.19
  14.6 2.5 all_gather.6
  17.1 0.9 pad_maximum_fusion.refs_0_
  18.7 69.3 %shard_map.172 = (bf16[8,8,32,1536]{3,2,1,0:T(8,128)(2,1)}, bf16[8,8,64,256]{3,2,1,0:T(8,128)(2,1)}, f32[8,8,2,256]{3,2,1,0:T(2,128)}) custom-call(bf16[8,32,1536]{2,1,0:T(8,128)(2,1)} %pad_maximum_fusion.refs_0_, bf16[8,64,256]{2,1,0:T(8,128)(2,1)} %bitcast.150, f32[8,2,256]{2,1,0:T(2,128)} %broadcast_in_dim.25.refs_2_), custom_call_target="tpu_custom_call" | custom-call | tf_op jit(solution)/shard_map/pallas_call | solution.py:213
  88.1 4.3 %convolution_multiply_fusion.1 = f32[192,1536]{1,0:T(8,128)S(1)} fusion(bf16[192,2048]{1,0:T(8,128)(2,1)S(1)} %all_gather.6, bf16[2048,1536]{1,0:T(8,128)(2,1)} %bitcast.168, f32[1536]{0:T(1024)S(1)} %pad_maximum_fusion.3), kind=kOutput, calls=%fused_computation.8 | convolution fusion | flops 1208254464 | bytes 8263680 | tf_op jit(solution)/shard_map/dot_general | solution.py:376
  92.5 1.0 copy-done.4
  93.8 2.4 copy.79
  98.8 1.3 fusion.17
  101.0 2.3 while.13
  103.3 2.0 multiply_reduce_fusion
  105.9 1.8 fusion.3
  107.8 1.0 copy.116
  108.7 3.7 %all-to-all-start = ((bf16[2,192,1024]{2,1,0:T(8,128)(2,1)}), bf16[2,192,1024]{2,1,0:T(8,128)(2,1)S(1)}, u32[]{:S(2)}, u32[]{:S(2)}) async-start(bf16[2,192,1024]{2,1,0:T(8,128)(2,1)} %bitcast.125), calls=%async_computation | async-start | bytes 1572864 | tf_op jit(solution)/shard_map/all_to_all | solution.py:409
  112.5 1.9 all-to-all-done
  114.7 2.6 psum.15
  118.2 37.6 %shard_map.173 = bf16[8,4,48,1024]{3,2,1,0:T(8,128)(2,1)} custom-call(bf16[4,48,1024]{2,1,0:T(8,128)(2,1)} %bitcast.147), custom_call_target="tpu_custom_call" | custom-call | tf_op jit(solution)/shard_map/pallas_call | solution.py:213
  155.9 2.5 convert_element_type.57
  158.3 1.6 copy.115
  160.0 1.7 copy-done
  161.6 1.5 convert_element_type.58
  163.1 55.3 %shard_map.174 = (bf16[8,2,128,512]{3,2,1,0:T(8,128)(2,1)}, bf16[8,2,256,256]{3,2,1,0:T(8,128)(2,1)}) custom-call(bf16[8,2,128,512]{3,2,1,0:T(8,128)(2,1)} %bitcast.137, bf16[8,2,256,256]{3,2,1,0:T(8,128)(2,1)} %bitcast.135), custom_call_target="tpu_custom_call" | custom-call | tf_op jit(solution)/shard_map/pallas_call | solution.py:291
  218.4 2.9 copy.82
  222.1 11.0 %multiply_convert_fusion = bf16[1536,2048]{1,0:T(8,128)(2,1)} fusion(bf16[2048,512]{1,0:T(8,128)(2,1)S(1)} %bitcast.145, f32[2048]{0:T(1024)S(1)} %bitcast.160, bf16[1536,2048]{1,0:T(8,128)(2,1)} %all-gather.2.cloned.1.call-done, bf16[2048,512]{1,0:T(8,128)(2,1)} %bitcast.169, f32[512]{0:T(512)S(1)} %dynamic_slice.15), kind=kOutput, calls=%fused_computation.2 | convolution fusion | flops 6451888128 | bytes 16787456 | tf_op jit(solution)/shard_map/ru,jud->rjd/dot_general | solution.py:473
  233.1 3.5 %copy.114 = bf16[192,2,8,1024]{3,2,0,1:T(8,128)(2,1)S(1)} copy(bf16[192,2,8,1024]{3,2,1,0:T(8,128)(2,1)} %bitcast.138) | data formatting | bytes 12582912 | tf_op jit(solution)/shard_map/reshape | solution.py:408
  236.6 10.0 %all_to_all.10 = bf16[2,1536,1024]{2,1,0:T(8,128)(2,1)} all-to-all(bf16[2,1536,1024]{2,1,0:T(8,128)(2,1)S(1)} %bitcast.132), channel_id=1, replica_groups=mesh['rep'=2,'fs'=8,'tp'=2] {'tp'}, dimensions={0} | all-to-all | bytes 12582912 | tf_op jit(solution)/shard_map/all_to_all | solution.py:409
  246.6 7.1 %reduce_sum.52 = bf16[1536,1024]{1,0:T(8,128)(2,1)} reduce(bf16[2,1536,1024]{2,1,0:T(8,128)(2,1)} %all_to_all.10, bf16[]{:T(256)} %constant.62.clone.1), dimensions={0}, to_apply=%region_8.10 | reduce | flops 1572864 | bytes 9437186 | tf_op jit(solution)/shard_map/reduce_sum | solution.py:410
  253.6 45.8 %shard_map.175 = f32[4,48,1024]{2,1,0:T(8,128)} custom-call(bf16[8,4,48,1024]{3,2,1,0:T(8,128)(2,1)} %bitcast.134), custom_call_target="tpu_custom_call" | custom-call | tf_op jit(solution)/shard_map/pallas_call | solution.py:347
  299.5 2.0 fusion.12
  (80 shorter events, 10.4 us)
Async XLA Ops:
  6.5 7.8 %copy-start.1 = (bf16[192,1024]{1,0:T(8,128)(2,1)S(1)}, bf16[192,1024]{1,0:T(8,128)(2,1)}, u32[]{:S(2)}) copy-start(bf16[192,1024]{1,0:T(8,128)(2,1)} %param.22) | copy-start | bytes 1179652
  6.5 7.0 %copy-start.5 = (f32[256,512]{1,0:T(8,128)S(1)}, f32[256,512]{1,0:T(8,128)}, u32[]{:S(2)}) copy-start(f32[256,512]{1,0:T(8,128)} %param.31) | copy-start | bytes 1572868
  6.5 7.1 %copy-start.6 = (f32[512,256]{1,0:T(8,128)S(1)}, f32[512,256]{1,0:T(8,128)}, u32[]{:S(2)}) copy-start(f32[512,256]{1,0:T(8,128)} %param.33) | copy-start | bytes 1572868
  6.5 7.8 %copy-start.10 = (f32[2048]{0:T(1024)S(1)}, f32[2048]{0:T(1024)}, u32[]{:S(2)}) copy-start(f32[2048]{0:T(1024)} %param.23) | copy-start | bytes 24580
  12.5 4.6 %copy-start.13 = (f32[256]{0:T(256)S(1)}, f32[256]{0:T(256)}, u32[]{:S(2)}) copy-start(f32[256]{0:T(256)} %param.38) | copy-start | bytes 3076
  12.5 4.6 %copy-start.14 = (f32[256]{0:T(256)S(1)}, f32[256]{0:T(256)}, u32[]{:S(2)}) copy-start(f32[256]{0:T(256)} %param.34) | copy-start | bytes 3076
  14.5 73.5 %copy-start.8 = (f32[512]{0:T(512)S(1)}, f32[512]{0:T(512)}, u32[]{:S(2)}) copy-start(f32[512]{0:T(512)} %param.32) | copy-start | bytes 6148
  14.5 73.5 %copy-start.9 = (f32[512]{0:T(512)S(1)}, f32[512]{0:T(512)}, u32[]{:S(2)}) copy-start(f32[512]{0:T(512)} %param.30) | copy-start | bytes 6148
  14.6 73.5 %copy-start.11 = (f32[256]{0:T(256)S(1)}, f32[256]{0:T(256)}, u32[]{:S(2)}) copy-start(f32[256]{0:T(256)} %param.28) | copy-start | bytes 3076
  14.6 73.5 %copy-start.12 = (f32[256]{0:T(256)S(1)}, f32[256]{0:T(256)}, u32[]{:S(2)}) copy-start(f32[256]{0:T(256)} %param.26) | copy-start | bytes 3076
  88.1 5.4 %copy-start.7 = (f32[4]{0:T(128)S(1)}, f32[4]{0:T(128)}, u32[]{:S(2)}) copy-start(f32[4]{0:T(128)} %param.39) | copy-start | bytes 52
  88.1 5.7 %copy-start.3 = (bf16[8,8,64,256]{3,2,1,0:T(8,128)(2,1)S(1)}, bf16[8,8,64,256]{3,2,1,0:T(8,128)(2,1)}, u32[]{:S(2)}) copy-start(bf16[8,8,64,256]{3,2,1,0:T(8,128)(2,1)} %get-tuple-element.40) | copy-start | bytes 6291460
  92.4 1.0 copy-start.4
  103.3 2.6 copy-start.2
  108.7 8.6 %dynamic-slice-start = ((f32[2048]{0:T(1024)}, s32[]{:T(128)}), f32[1024]{0:T(1024)S(1)}, s32[]{:S(2)}) async-start(f32[2048]{0:T(1024)} %param.24, s32[]{:T(128)} %select_n.15), calls=%async_computation.3 | async-start | bytes 8704 | tf_op jit(solution)/shard_map/dynamic_slice | solution.py:366
  108.7 5.6 %all-to-all-start = ((bf16[2,192,1024]{2,1,0:T(8,128)(2,1)}), bf16[2,192,1024]{2,1,0:T(8,128)(2,1)S(1)}, u32[]{:S(2)}, u32[]{:S(2)}) async-start(bf16[2,192,1024]{2,1,0:T(8,128)(2,1)} %bitcast.125), calls=%async_computation | async-start | bytes 1572864 | tf_op jit(solution)/shard_map/all_to_all | solution.py:409
  112.4 109.7 %all-gather.2.cloned.1.call-start = ((), (), s32[]{:S(2)}) async-start(), calls=%async_computation.2 | async-start | bytes 9437184 | tf_op jit(solution)/shard_map/all_gather | solution.py:372
  158.3 3.3 %copy-start = (f32[4096,256]{1,0:T(8,128)S(1)}, f32[4096,256]{1,0:T(8,128)}, u32[]{:S(2)}) copy-start(f32[4096,256]{1,0:T(8,128)} %param.37) | copy-start | bytes 12582916
Sparse Core Ops, SparseCore 0:
  156.0 15.2 all-gather.1

commit v3 on v2

--- a/solution.py
+++ b/solution.py
@@ -464,7 +464,7 @@
     first = mixer(activations, mix_gain, four, four_scale, out_full, scales[0], log_decay)
     half_rows = norm_half(first, mlp_gain)
     normed_two = tp_columns(
-        ring_gather([half_rows.reshape(4, -1, half_rows.shape[1])], n, False, 2)[0].reshape(
+        ring_gather([half_rows.reshape(6, -1, half_rows.shape[1])], n, False, 2)[0].reshape(
             -1, half_rows.shape[1]
         )
     )
@@ -473,7 +473,7 @@
     share = jnp.einsum("ru,jud->rjd", hidden, down_mine, preferred_element_type=jnp.float32)
     share = share.reshape(share.shape[0], -1) * scales[1]
     pair = tp_sum(share.astype(bf)).astype(bf)
-    shares = pair.reshape(n, 4, -1, first.shape[1])
+    shares = pair.reshape(n, 12, -1, first.shape[1])
     channel = ring_sum(shares, n, 3).reshape(first.shape)
     return (first.astype(jnp.float32) + channel).astype(bf)
 

time: 309 us -> 315 us (1.019)
  Pallas kernels: 208 us -> 214 us
    pallas_call x1, Pallas kernels: 55.3 us -> 62.3 us  [spread(): pl.pallas_call(functools.partial(spread_kernel, n, count), out_shape=[jax...]
  transfers between devices with their start and end apart: 2 -> 2, of which waited for: 1 -> 1; matrix products, arithmetic and copies ran while one was open for 3% -> 3% of each run, Pallas kernels for 18% -> 20%
where the time goes in v3:
time: 315 us; the launch traced here: 314 us
  Pallas kernels  214 us (68%)
  other arithmetic  23.3 us (7%)
  matrix products  22.1 us (7%)
  blocking collectives  17.8 us (6%)
  local copies, waits for them, and re-layouts  17.7 us (6%)
  between operations  13.8 us (4%)
  starting transfers between devices  3.71 us (1%)
    pallas_call x2, Pallas kernels, ring_gather(): pl.pallas_call(functools.partial(ring_gather_kernel, n, count, shared), o...  104 us
    pallas_call x1, Pallas kernels, spread(): pl.pallas_call(functools.partial(spread_kernel, n, count), out_shape=[jax...  62.3 us
    pallas_call x1, Pallas kernels, ring_sum(): pl.pallas_call(functools.partial(ring_sum_kernel, n), out_shape=jax.Shape...  47.4 us
    dot_general x1, matrix products, on_device(): jnp.einsum('ru,jud->rjd', hidden, down_mine, preferred_element_type=jnp.f...  11 us
    all_to_all x1, blocking collectives, tp_sum(): arrived = lax.all_to_all(spread, 'tp', 0, 0, tiled=True)  9.99 us
    reduce_sum x2, other arithmetic, tp_sum(): return jnp.sum(arrived.astype(jnp.float32), axis=0)  7.21 us
  transfers between devices with their start and end apart: 2, of which 1 were waited for; matrix products, arithmetic and copies ran while one was open for 3% of the time, Pallas kernels for 20%

profile of v3, /device:TPU:0, one launch (start us, length us, event | category | flops | bytes accessed | tf_op | source)
XLA Modules:
  0.0 314.4 jit_solution(13235339665366902897)
XLA Ops:
  6.6 1.2 fusion.5
  7.9 2.6 psum.14
  10.5 1.0 convert.17
  11.5 1.0 convert.18
  12.5 1.1 convert.19
  14.6 2.5 all_gather.6
  17.1 0.9 pad_maximum_fusion.refs_0_
  18.7 69.3 %shard_map.172 = (bf16[8,8,32,1536]{3,2,1,0:T(8,128)(2,1)}, bf16[8,8,64,256]{3,2,1,0:T(8,128)(2,1)}, f32[8,8,2,256]{3,2,1,0:T(2,128)}) custom-call(bf16[8,32,1536]{2,1,0:T(8,128)(2,1)} %pad_maximum_fusion.refs_0_, bf16[8,64,256]{2,1,0:T(8,128)(2,1)} %bitcast.150, f32[8,2,256]{2,1,0:T(2,128)} %broadcast_in_dim.25.refs_2_), custom_call_target="tpu_custom_call" | custom-call | tf_op jit(solution)/shard_map/pallas_call | solution.py:213
  88.1 4.3 %convolution_multiply_fusion.1 = f32[192,1536]{1,0:T(8,128)S(1)} fusion(bf16[192,2048]{1,0:T(8,128)(2,1)S(1)} %all_gather.6, bf16[2048,1536]{1,0:T(8,128)(2,1)} %bitcast.168, f32[1536]{0:T(1024)S(1)} %pad_maximum_fusion.3), kind=kOutput, calls=%fused_computation.8 | convolution fusion | flops 1208254464 | bytes 8263680 | tf_op jit(solution)/shard_map/dot_general | solution.py:376
  92.5 1.0 copy-done.4
  93.8 2.4 copy.79
  98.8 1.3 fusion.17
  101.0 2.3 while.13
  103.3 2.0 multiply_reduce_fusion
  105.9 1.8 fusion.3
  107.8 1.0 copy.116
  108.7 3.7 %all-to-all-start = ((bf16[2,192,1024]{2,1,0:T(8,128)(2,1)}), bf16[2,192,1024]{2,1,0:T(8,128)(2,1)S(1)}, u32[]{:S(2)}, u32[]{:S(2)}) async-start(bf16[2,192,1024]{2,1,0:T(8,128)(2,1)} %bitcast.125), calls=%async_computation | async-start | bytes 1572864 | tf_op jit(solution)/shard_map/all_to_all | solution.py:409
  112.5 1.9 all-to-all-done
  114.7 2.6 psum.15
  118.2 35.1 %shard_map.173 = bf16[8,6,32,1024]{3,2,1,0:T(8,128)(2,1)} custom-call(bf16[6,32,1024]{2,1,0:T(8,128)(2,1)} %bitcast.147), custom_call_target="tpu_custom_call" | custom-call | tf_op jit(solution)/shard_map/pallas_call | solution.py:213
  153.3 2.5 convert_element_type.57
  155.8 1.6 copy.115
  157.5 1.6 copy-done
  159.1 1.5 convert_element_type.58
  160.6 62.3 %shard_map.174 = (bf16[8,2,128,512]{3,2,1,0:T(8,128)(2,1)}, bf16[8,2,256,256]{3,2,1,0:T(8,128)(2,1)}) custom-call(bf16[8,2,128,512]{3,2,1,0:T(8,128)(2,1)} %bitcast.137, bf16[8,2,256,256]{3,2,1,0:T(8,128)(2,1)} %bitcast.135), custom_call_target="tpu_custom_call" | custom-call | tf_op jit(solution)/shard_map/pallas_call | solution.py:291
  222.9 2.9 copy.82
  226.6 11.0 %multiply_convert_fusion = bf16[1536,2048]{1,0:T(8,128)(2,1)} fusion(bf16[2048,512]{1,0:T(8,128)(2,1)S(1)} %bitcast.145, f32[2048]{0:T(1024)S(1)} %bitcast.160, bf16[1536,2048]{1,0:T(8,128)(2,1)} %all-gather.2.cloned.1.call-done, bf16[2048,512]{1,0:T(8,128)(2,1)} %bitcast.169, f32[512]{0:T(512)S(1)} %dynamic_slice.15), kind=kOutput, calls=%fused_computation.2 | convolution fusion | flops 6451888128 | bytes 16787456 | tf_op jit(solution)/shard_map/ru,jud->rjd/dot_general | solution.py:473
  237.6 3.5 %copy.114 = bf16[192,2,8,1024]{3,2,0,1:T(8,128)(2,1)S(1)} copy(bf16[192,2,8,1024]{3,2,1,0:T(8,128)(2,1)} %bitcast.138) | data formatting | bytes 12582912 | tf_op jit(solution)/shard_map/reshape | solution.py:408
  241.1 10.0 %all_to_all.10 = bf16[2,1536,1024]{2,1,0:T(8,128)(2,1)} all-to-all(bf16[2,1536,1024]{2,1,0:T(8,128)(2,1)S(1)} %bitcast.132), channel_id=1, replica_groups=mesh['rep'=2,'fs'=8,'tp'=2] {'tp'}, dimensions={0} | all-to-all | bytes 12582912 | tf_op jit(solution)/shard_map/all_to_all | solution.py:409
  251.1 7.1 %reduce_sum.52 = bf16[1536,1024]{1,0:T(8,128)(2,1)} reduce(bf16[2,1536,1024]{2,1,0:T(8,128)(2,1)} %all_to_all.10, bf16[]{:T(256)} %constant.62.clone.1), dimensions={0}, to_apply=%region_8.10 | reduce | flops 1572864 | bytes 9437186 | tf_op jit(solution)/shard_map/reduce_sum | solution.py:410
  258.1 47.4 %shard_map.175 = f32[12,16,1024]{2,1,0:T(8,128)} custom-call(bf16[8,12,16,1024]{3,2,1,0:T(8,128)(2,1)} %bitcast.134), custom_call_target="tpu_custom_call" | custom-call | tf_op jit(solution)/shard_map/pallas_call | solution.py:347
  305.6 2.0 fusion.12
  (80 shorter events, 10.4 us)
Async XLA Ops:
  6.5 7.8 %copy-start.1 = (bf16[192,1024]{1,0:T(8,128)(2,1)S(1)}, bf16[192,1024]{1,0:T(8,128)(2,1)}, u32[]{:S(2)}) copy-start(bf16[192,1024]{1,0:T(8,128)(2,1)} %param.22) | copy-start | bytes 1179652
  6.5 7.0 %copy-start.5 = (f32[256,512]{1,0:T(8,128)S(1)}, f32[256,512]{1,0:T(8,128)}, u32[]{:S(2)}) copy-start(f32[256,512]{1,0:T(8,128)} %param.31) | copy-start | bytes 1572868
  6.5 7.1 %copy-start.6 = (f32[512,256]{1,0:T(8,128)S(1)}, f32[512,256]{1,0:T(8,128)}, u32[]{:S(2)}) copy-start(f32[512,256]{1,0:T(8,128)} %param.33) | copy-start | bytes 1572868
  6.5 7.8 %copy-start.10 = (f32[2048]{0:T(1024)S(1)}, f32[2048]{0:T(1024)}, u32[]{:S(2)}) copy-start(f32[2048]{0:T(1024)} %param.23) | copy-start | bytes 24580
  12.5 4.6 %copy-start.13 = (f32[256]{0:T(256)S(1)}, f32[256]{0:T(256)}, u32[]{:S(2)}) copy-start(f32[256]{0:T(256)} %param.38) | copy-start | bytes 3076
  12.5 4.6 %copy-start.14 = (f32[256]{0:T(256)S(1)}, f32[256]{0:T(256)}, u32[]{:S(2)}) copy-start(f32[256]{0:T(256)} %param.34) | copy-start | bytes 3076
  14.5 73.5 %copy-start.8 = (f32[512]{0:T(512)S(1)}, f32[512]{0:T(512)}, u32[]{:S(2)}) copy-start(f32[512]{0:T(512)} %param.32) | copy-start | bytes 6148
  14.5 73.5 %copy-start.9 = (f32[512]{0:T(512)S(1)}, f32[512]{0:T(512)}, u32[]{:S(2)}) copy-start(f32[512]{0:T(512)} %param.30) | copy-start | bytes 6148
  14.6 73.5 %copy-start.11 = (f32[256]{0:T(256)S(1)}, f32[256]{0:T(256)}, u32[]{:S(2)}) copy-start(f32[256]{0:T(256)} %param.28) | copy-start | bytes 3076
  14.6 73.5 %copy-start.12 = (f32[256]{0:T(256)S(1)}, f32[256]{0:T(256)}, u32[]{:S(2)}) copy-start(f32[256]{0:T(256)} %param.26) | copy-start | bytes 3076
  88.1 5.4 %copy-start.7 = (f32[4]{0:T(128)S(1)}, f32[4]{0:T(128)}, u32[]{:S(2)}) copy-start(f32[4]{0:T(128)} %param.39) | copy-start | bytes 52
  88.1 5.7 %copy-start.3 = (bf16[8,8,64,256]{3,2,1,0:T(8,128)(2,1)S(1)}, bf16[8,8,64,256]{3,2,1,0:T(8,128)(2,1)}, u32[]{:S(2)}) copy-start(bf16[8,8,64,256]{3,2,1,0:T(8,128)(2,1)} %get-tuple-element.40) | copy-start | bytes 6291460
  92.4 1.0 copy-start.4
  103.3 2.6 copy-start.2
  108.7 8.6 %dynamic-slice-start = ((f32[2048]{0:T(1024)}, s32[]{:T(128)}), f32[1024]{0:T(1024)S(1)}, s32[]{:S(2)}) async-start(f32[2048]{0:T(1024)} %param.24, s32[]{:T(128)} %select_n.15), calls=%async_computation.3 | async-start | bytes 8704 | tf_op jit(solution)/shard_map/dynamic_slice | solution.py:366
  108.7 5.6 %all-to-all-start = ((bf16[2,192,1024]{2,1,0:T(8,128)(2,1)}), bf16[2,192,1024]{2,1,0:T(8,128)(2,1)S(1)}, u32[]{:S(2)}, u32[]{:S(2)}) async-start(bf16[2,192,1024]{2,1,0:T(8,128)(2,1)} %bitcast.125), calls=%async_computation | async-start | bytes 1572864 | tf_op jit(solution)/shard_map/all_to_all | solution.py:409
  112.4 114.2 %all-gather.2.cloned.1.call-start = ((), (), s32[]{:S(2)}) async-start(), calls=%async_computation.2 | async-start | bytes 9437184 | tf_op jit(solution)/shard_map/all_gather | solution.py:372
  155.8 3.3 %copy-start = (f32[4096,256]{1,0:T(8,128)S(1)}, f32[4096,256]{1,0:T(8,128)}, u32[]{:S(2)}) copy-start(f32[4096,256]{1,0:T(8,128)} %param.37) | copy-start | bytes 12582916
Sparse Core Ops, SparseCore 0:
  153.5 15.4 all-gather.1
